TPU v7x, 32 devices: a whole 2x2x4 slice. The times are simulated.
32 devices in a mesh: sp: 8 (over z, core), tp: 4 (over y, x).
Axes of the slice: x: 2, y: 2, z: 4, core: 2. Of those that a mesh axis runs over, the one named last changes fastest.
Arguments:
- queries: bfloat16 [2048, 1024], P('sp', 'tp'), may hold values from -250 to 250
- keys_values: bfloat16 [2, 2048, 256], P(None, 'sp'), may hold values from -8 to 8
- sink_logits: float32 [16], P('tp'), may hold values from 1 to 5
- proj_weight: bfloat16 [1024, 2048], P('tp'), may hold values from -0.75 to 0.75
- residual: bfloat16 [2048, 2048], P('sp', 'tp'), may hold values from -6 to 6
- norm_gain: float32 [2048], replicated, may hold values from 0.1 to 1.9
- routes: int32 [2048, 2], P('sp'), may hold values from 0 to 7, all different within a row; in each aligned block of 256 rows (0 to 255, 256 to 511, ...) at most 128 rows name the same one
- route_weights: float32 [2048, 2], P('sp'), may hold values from 0.2 to 1
- gate_weight: bfloat16 [8, 2048, 2048], P('sp', None, 'tp'), may hold values from -0.125 to 0.125
- up_weight: bfloat16 [8, 2048, 2048], P('sp', None, 'tp'), may hold values from -0.125 to 0.125
- down_weight: bfloat16 [8, 2048, 2048], P('sp', None, 'tp'), may hold values from -0.125 to 0.125
- shared_gate: bfloat16 [2048, 2048], P(None, 'tp'), may hold values from -0.125 to 0.125
- shared_up: bfloat16 [2048, 2048], P(None, 'tp'), may hold values from -0.125 to 0.125
- shared_down: bfloat16 [2048, 2048], P(None, 'tp'), may hold values from -0.125 to 0.125
Outputs:
- output: bfloat16 [2048, 2048], P('sp', 'tp')
Inputs may be any that keep to these rules, and one draw needn't show every extreme that they name: `routes`: the 2 experts of a position differ. In each aligned block of 256 positions no expert is named by more than 128 positions, and in some block one expert is named by exactly 128.
All inputs are finite; a program needn't handle non-finite values.
Results may differ from a plain program's by a relative error of at most 0.0067.
Values may be sent and summed in bfloat16 or wider, within the bound.
A program may use at most 64 MiB of HBM per device.

v0:
```python
import jax
import jax.numpy as jnp
from jax import lax
from jax.sharding import PartitionSpec as P

D = 2048
HEADS = 16
KV_HEADS = 4
HEAD_WIDTH = 64
WINDOW = 128
TOP_K = 2
EXP_DEV = 1
TOK_DEV = 256
norm_eps = 1e-06


def passed_along(value, axis, steps):
    count = lax.axis_size(axis)
    initial, last = (max(0, -steps), min(count, count - steps))
    return lax.ppermute(value, axis, [(source, source + steps) for source in range(initial, last)])


def per_device(
    queries,
    keys_values,
    sink_logits,
    proj_weight,
    residual,
    norm_gain,
    routes,
    route_weights,
    gate_weight,
    up_weight,
    down_weight,
    shared_gate,
    shared_up,
    shared_down,
):
    tp_index = lax.axis_index("tp")
    sp_index = lax.axis_index("sp")
    sp_count = lax.axis_size("sp")
    tp_count = lax.axis_size("tp")
    heads_here = sink_logits.shape[0]
    col_width = residual.shape[1]
    blocks = TOK_DEV // WINDOW
    kv_group = HEADS // KV_HEADS
    earlier_keys = passed_along(keys_values[:, TOK_DEV - WINDOW :, :], "sp", 1)
    extended = jnp.concatenate([earlier_keys, keys_values], axis=1)
    extended = extended.reshape(2, TOK_DEV + WINDOW, KV_HEADS, HEAD_WIDTH)
    head_ids = tp_index * heads_here + jnp.arange(heads_here, dtype=jnp.int32)
    chosen = jnp.take(extended, head_ids // kv_group, axis=2)
    earlier = chosen[:, :TOK_DEV].reshape(2, blocks, WINDOW, heads_here, HEAD_WIDTH)
    later = chosen[:, WINDOW:].reshape(2, blocks, WINDOW, heads_here, HEAD_WIDTH)
    banded = jnp.concatenate([earlier, later], axis=2)
    query_blocks = queries.reshape(blocks, WINDOW, heads_here, HEAD_WIDTH)
    score_matrix = jnp.einsum(
        "bqhd,bkhd->bhqk", query_blocks, banded[0], preferred_element_type=jnp.float32
    ) * HEAD_WIDTH ** (-0.5)
    query_pos = jnp.arange(WINDOW, dtype=jnp.int32)[:, None]
    key_pos = jnp.arange(2 * WINDOW, dtype=jnp.int32)[None, :]
    distance = WINDOW + query_pos - key_pos
    absolute = (
        sp_index * TOK_DEV
        + jnp.arange(blocks, dtype=jnp.int32)[:, None, None] * WINDOW
        - WINDOW
        + key_pos[None]
    )
    allowed = (distance >= 0)[None] & (distance < WINDOW)[None] & (absolute >= 0)
    masked = jnp.where(allowed[:, None], score_matrix, -jnp.inf)
    sink_value = sink_logits[None, :, None, None]
    highest = jnp.maximum(jnp.max(masked, axis=-1, keepdims=True), sink_value)
    weights_exp = jnp.exp(masked - highest)
    denominator = jnp.sum(weights_exp, axis=-1, keepdims=True) + jnp.exp(sink_value - highest)
    softmax_weights = (weights_exp / denominator).astype(jnp.bfloat16)
    attended_values = jnp.einsum(
        "bhqk,bkhd->bqhd", softmax_weights, banded[1], preferred_element_type=jnp.float32
    )
    attended_values = attended_values.astype(jnp.bfloat16).reshape(TOK_DEV, heads_here * HEAD_WIDTH)
    attended_all = lax.all_gather(attended_values, "tp", axis=1, tiled=True)
    weight_rows = proj_weight.shape[0]
    column_share = lax.all_to_all(
        proj_weight.reshape(weight_rows, tp_count, col_width),
        "tp",
        split_axis=1,
        concat_axis=0,
        tiled=True,
    )
    column_share = column_share.reshape(HEADS * HEAD_WIDTH, col_width)
    feature_sum = jnp.dot(attended_all, column_share, preferred_element_type=jnp.float32)
    stream_cols = (feature_sum + residual.astype(jnp.float32)).astype(jnp.bfloat16)
    stream_rows = lax.all_gather(stream_cols, "tp", axis=1, tiled=True)
    gate_eff = (norm_gain[None, :, None] * gate_weight.astype(jnp.float32)).astype(jnp.bfloat16)
    up_eff = (norm_gain[None, :, None] * up_weight.astype(jnp.float32)).astype(jnp.bfloat16)
    shared_gate_eff = (norm_gain[:, None] * shared_gate.astype(jnp.float32)).astype(jnp.bfloat16)
    shared_up_eff = (norm_gain[:, None] * shared_up.astype(jnp.float32)).astype(jnp.bfloat16)
    experts_total = EXP_DEV * sp_count
    capacity = 2 * TOK_DEV * TOP_K // experts_total
    rows_per_expert = sp_count * capacity
    flat_routes = routes.reshape(-1)
    onehot = (flat_routes[:, None] == jnp.arange(experts_total, dtype=jnp.int32)[None, :]).astype(
        jnp.int32
    )
    before = jnp.cumsum(onehot, axis=0) - onehot
    slot_rank = jnp.sum(before * onehot, axis=1)
    slot_index = (
        flat_routes % EXP_DEV * rows_per_expert + flat_routes // EXP_DEV * capacity + slot_rank
    )
    token_of = jnp.arange(TOK_DEV * TOP_K, dtype=jnp.int32) // TOP_K
    slot_owner = (
        jnp.full((EXP_DEV * rows_per_expert,), TOK_DEV, jnp.int32).at[slot_index].set(token_of)
    )
    picked_rows = jnp.take(stream_rows, slot_owner, axis=0, mode="fill", fill_value=0)
    arrived = lax.all_to_all(
        picked_rows.reshape(EXP_DEV, sp_count, capacity, stream_rows.shape[1]),
        "sp",
        split_axis=1,
        concat_axis=1,
        tiled=True,
    )
    arrived = arrived.reshape(EXP_DEV, rows_per_expert, D)
    routed_squares = jnp.sum(jnp.square(arrived.astype(jnp.float32)), axis=-1)
    gate_sum = jnp.einsum("erd,edf->erf", arrived, gate_eff, preferred_element_type=jnp.float32)
    up_sum = jnp.einsum("erd,edf->erf", arrived, up_eff, preferred_element_type=jnp.float32)
    own_squares = jnp.sum(jnp.square(stream_rows.astype(jnp.float32)), axis=-1)
    shared_gate_sum = jnp.dot(stream_rows, shared_gate_eff, preferred_element_type=jnp.float32)
    shared_up_sum = jnp.dot(stream_rows, shared_up_eff, preferred_element_type=jnp.float32)
    routed_scale = lax.rsqrt(routed_squares / D + norm_eps)[..., None]
    own_scale = lax.rsqrt(own_squares / D + norm_eps)[:, None]
    hidden = (jax.nn.silu(routed_scale * gate_sum) * (routed_scale * up_sum)).astype(jnp.bfloat16)
    shared_hidden = (jax.nn.silu(own_scale * shared_gate_sum) * (own_scale * shared_up_sum)).astype(
        jnp.bfloat16
    )
    routed_piece = lax.all_gather(hidden, "tp", axis=2, tiled=True)
    own_piece = lax.all_gather(shared_hidden[None], "tp", axis=2, tiled=True)
    expert_out = jnp.einsum(
        "erf,efd->erd", routed_piece, down_weight, preferred_element_type=jnp.float32
    )
    shared_out = jnp.dot(own_piece[0], shared_down, preferred_element_type=jnp.float32)
    outgoing = expert_out.astype(jnp.bfloat16).reshape(EXP_DEV, sp_count, capacity, col_width)
    returned = lax.all_to_all(outgoing, "sp", split_axis=1, concat_axis=1, tiled=True).reshape(
        EXP_DEV * rows_per_expert, col_width
    )
    picked = jnp.take(returned, slot_index, axis=0).reshape(TOK_DEV, TOP_K, col_width)
    routed_sum = jnp.einsum("nk,nkd->nd", route_weights, picked.astype(jnp.float32))
    return (stream_cols.astype(jnp.float32) + shared_out + routed_sum).astype(jnp.bfloat16)


def solution(mesh):
    placed = (
        P("sp", "tp"),
        P(None, "sp", None),
        P("tp"),
        P("tp", None),
        P("sp", "tp"),
        P(),
        P("sp", None),
        P("sp", None),
        P("sp", None, "tp"),
        P("sp", None, "tp"),
        P("sp", None, "tp"),
        P(None, "tp"),
        P(None, "tp"),
        P(None, "tp"),
    )
    return jax.shard_map(
        per_device, mesh=mesh, in_specs=placed, out_specs=P("sp", "tp"), check_vma=False
    )
```

profile of v0, /device:TPU:0, one launch (start us, length us, event | category | flops | bytes accessed | tf_op | source)
XLA Modules:
  0.0 293.3 jit_solution(9455327325811044780)
XLA Ops:
  7.8 3.2 %collective-permute-start = (bf16[2,128,256]{1,2,0:T(8,128)(2,1)S(1)}, bf16[2,128,256]{1,2,0:T(8,128)(2,1)}, u32[]{:S(2)}, u32[]{:S(2)}) collective-permute-start(bf16[2,128,256]{1,2,0:T(8,128)(2,1)S(1)} %slice.34), channel_id=1, source_target_pairs={{0,4},{4,8},{8,12},{12,16},{16,20},{20,24},{24,28},{1,5},{5,9},{9,... | collective-permute-start | bytes 393224 | tf_op jit(solution)/shard_map/ppermute | solution.py:20
  11.0 2.3 copy.73
  13.3 4.5 %all-to-all-start = ((bf16[256,4,512]{0,2,1:T(8,128)(2,1)}), bf16[256,4,512]{0,2,1:T(8,128)(2,1)S(1)}, u32[]{:S(2)}, u32[]{:S(2)}) async-start(bf16[256,4,512]{0,2,1:T(8,128)(2,1)} %bitcast.91), calls=%async_computation | async-start | bytes 2097152 | tf_op jit(solution)/shard_map/all_to_all | solution.py:81
  20.7 1.4 gather_fusion
  27.6 1.5 fusion.48
  30.0 12.7 %all_gather.12 = bf16[256,1024]{0,1:T(8,128)(2,1)} all-gather(bf16[256,256]{0,1:T(8,128)(2,1)S(1)} %bitcast.95), channel_id=1, replica_groups=mesh['sp'=8,'tp'=4] {'tp'}, dimensions={1}, use_global_device_ids=true | all-gather | bytes 655360 | tf_op jit(solution)/shard_map/all_gather | solution.py:79
  42.7 1.3 copy.74
  44.0 2.6 fusion.25
  48.9 2.4 scatter_custom_fusion
  51.4 20.4 %all-gather.6.cloned.1.call-done = bf16[256,2048]{1,0:T(8,128)(2,1)} async-done(((bf16[256,512]{1,0:T(8,128)(2,1)}), bf16[256,2048]{1,0:T(8,128)(2,1)}) %all-gather.6.cloned.1.call-update) | async-done | bytes 1048592 | tf_op jit(solution)/shard_map/all_gather | solution.py:91
  71.8 10.2 %gather_fusion.1 = bf16[1024,2048]{1,0:T(8,128)(2,1)} fusion(bf16[256,2048]{1,0:T(8,128)(2,1)} %all-gather.6.cloned.1.call-done, s32[1024]{0:T(1024)S(1)} %fusion.39), kind=kCustom, calls=%fused_computation.1 | custom fusion | bytes 8392704 | tf_op jit(solution)/shard_map/jit(_take)/gather | solution.py:112
  82.0 2.5 broadcast_select_fusion
  84.5 98.4 %all_to_all.25 = bf16[1,8,128,2048]{3,2,0,1:T(8,128)(2,1)S(1)} all-to-all(bf16[1,8,128,2048]{3,2,0,1:T(8,128)(2,1)S(1)} %broadcast_select_fusion), channel_id=1, replica_groups=mesh['sp'=8,'tp'=4] {'sp'}, dimensions={1} | all-to-all | bytes 8388608 | tf_op jit(solution)/shard_map/all_to_all | solution.py:113
  184.5 2.4 fusion.3
  186.9 3.7 %multiply_convert_fusion.6 = bf16[1024,512]{1,0:T(8,128)(2,1)} fusion(f32[1024,512]{1,0:T(8,128)S(1)} %fusion.3, bf16[1024,2048]{1,0:T(8,128)(2,1)S(1)} %bitcast.89, bf16[1,2048,512]{2,1,0:T(8,128)(2,1)S(1)} %copy-done.11, f32[2048]{0:T(1024)S(1)} %copy-done.14, f32[1024]{0:T(1024)S(1)} %rsqrt_bitcast_fusion), kind=kOutput, calls=%fused_computation.18 | convolution fusion | flops 2154823680 | bytes 9449472 | tf_op jit(solution)/shard_map/erd,edf->erf/dot_general | solution.py:123
  191.0 50.3 %all-gather.10.cloned.1.call-done = bf16[1024,2048]{1,0:T(8,128)(2,1)} async-done(((bf16[1024,512]{1,0:T(8,128)(2,1)}), bf16[1024,2048]{1,0:T(8,128)(2,1)}) %all-gather.10.cloned.1.call-update) | async-done | bytes 4194320 | tf_op jit(solution)/shard_map/all_gather | solution.py:133
  241.3 5.5 %fusion.16 = bf16[1024,512]{1,0:T(8,128)(2,1)} fusion(bf16[1024,2048]{1,0:T(8,128)(2,1)} %all-gather.10.cloned.1.call-done, bf16[1,2048,512]{2,1,0:T(8,128)(2,1)S(1)} %copy-done), kind=kOutput, calls=%fused_computation.24 | convolution fusion | flops 2148007936 | bytes 7340032 | tf_op jit(solution)/shard_map/erf,efd->erd/dot_general | solution.py:135
  246.8 4.6 %all-to-all-start.2 = ((bf16[1,8,128,512]{3,2,0,1:T(8,128)(2,1)}), bf16[1,8,128,512]{3,2,0,1:T(8,128)(2,1)}, u32[]{:S(2)}, u32[]{:S(2)}) async-start(bf16[1,8,128,512]{3,2,0,1:T(8,128)(2,1)} %bitcast.93), calls=%async_computation.2 | async-start | bytes 2097152 | tf_op jit(solution)/shard_map/all_to_all | solution.py:140
  251.4 2.6 fusion.23
  254.0 1.6 fusion.27
  256.3 21.8 %all-to-all-done.2 = bf16[1,8,128,512]{3,2,0,1:T(8,128)(2,1)} async-done(((bf16[1,8,128,512]{3,2,0,1:T(8,128)(2,1)}), bf16[1,8,128,512]{3,2,0,1:T(8,128)(2,1)}, u32[]{:S(2)}, u32[]{:S(2)}) %all-to-all-start.2) | async-done | bytes 1048608 | tf_op jit(solution)/shard_map/all_to_all | solution.py:140
  278.0 3.3 %gather_fusion.2 = bf16[512,512]{1,0:T(8,128)(2,1)S(1)} fusion(bf16[1024,512]{1,0:T(8,128)(2,1)} %bitcast.25, s32[1024]{0:T(1024)S(1)} %pad_clamp_fusion), kind=kCustom, calls=%fused_computation.2 | custom fusion | bytes 1050624 | tf_op jit(solution)/shard_map/jit(_take)/gather | solution.py:143
  281.6 1.8 fusion.30
  283.4 3.4 %fusion.26 = bf16[256,512]{1,0:T(8,128)(2,1)} fusion(bf16[256,2048]{1,0:T(8,128)(2,1)} %all-gather.8.cloned.1.call-done, bf16[2048,512]{1,0:T(8,128)(2,1)} %param.27, f32[256,1,512]{2,1,0:T(1,128)} %fusion.30, bf16[256,512]{1,0:T(8,128)(2,1)S(1)} %copy-done.3), kind=kOutput, calls=%fused_computation.35 | convolution fusion | flops 537395200 | bytes 4194304 | tf_op jit(solution)/shard_map/dot_general | solution.py:138
  (90 shorter events, 15.6 us)
Async XLA Ops:
  6.5 234.7 %copy-start = (bf16[1,2048,512]{2,1,0:T(8,128)(2,1)S(1)}, bf16[1,2048,512]{2,1,0:T(8,128)(2,1)}, u32[]{:S(2)}) copy-start(bf16[1,2048,512]{2,1,0:T(8,128)(2,1)} %param.24) | copy-start | bytes 6291460
  7.8 5.5 %copy-start.2 = (bf16[2,256,256]{1,2,0:T(8,128)(2,1)}, bf16[2,256,256]{1,2,0:T(8,128)(2,1)S(1)}, u32[]{:S(2)}) copy-start(bf16[2,256,256]{1,2,0:T(8,128)(2,1)S(1)} %copy.63) | copy-start | bytes 786436
  7.8 10.9 %copy-start.4 = (bf16[256,256]{1,0:T(8,128)(2,1)S(1)}, bf16[256,256]{1,0:T(8,128)(2,1)}, u32[]{:S(2)}) copy-start(bf16[256,256]{1,0:T(8,128)(2,1)} %param.14) | copy-start | bytes 393220
  7.8 11.8 %collective-permute-start = (bf16[2,128,256]{1,2,0:T(8,128)(2,1)S(1)}, bf16[2,128,256]{1,2,0:T(8,128)(2,1)}, u32[]{:S(2)}, u32[]{:S(2)}) collective-permute-start(bf16[2,128,256]{1,2,0:T(8,128)(2,1)S(1)} %slice.34), channel_id=1, source_target_pairs={{0,4},{4,8},{8,12},{12,16},{16,20},{20,24},{24,28},{1,5},{5,9},{9,... | collective-permute-start | bytes 393224 | tf_op jit(solution)/shard_map/ppermute | solution.py:20
  13.3 29.4 %all-to-all-start = ((bf16[256,4,512]{0,2,1:T(8,128)(2,1)}), bf16[256,4,512]{0,2,1:T(8,128)(2,1)S(1)}, u32[]{:S(2)}, u32[]{:S(2)}) async-start(bf16[256,4,512]{0,2,1:T(8,128)(2,1)} %bitcast.91), calls=%async_computation | async-start | bytes 2097152 | tf_op jit(solution)/shard_map/all_to_all | solution.py:81
  17.8 54.0 %all-gather.6.cloned.1.call-start = ((), (), s32[]{:S(2)}) async-start(), calls=%async_computation.3 | async-start | bytes 1310720 | tf_op jit(solution)/shard_map/all_gather | solution.py:91
  22.0 5.6 %copy-start.6 = (pred[2,128,256]{1,2,0:T(8,128)(4,1)S(1)}, pred[2,128,256]{1,2,0:T(8,128)(4,1)}, u32[]{:S(2)}) copy-start(pred[2,128,256]{1,2,0:T(8,128)(4,1)} %broadcast_and_fusion) | copy-start | bytes 196612
  24.0 5.1 %copy-start.9 = (f32[4]{0:T(128)S(1)}, f32[4]{0:T(128)}, u32[]{:S(2)}) copy-start(f32[4]{0:T(128)} %param.16) | copy-start | bytes 52
  27.6 1.8 copy-start.5
  29.8 14.3 %copy-start.13 = (bf16[256,512]{1,0:T(8,128)(2,1)S(1)}, bf16[256,512]{1,0:T(8,128)(2,1)}, u32[]{:S(2)}) copy-start(bf16[256,512]{1,0:T(8,128)(2,1)} %param.18) | copy-start | bytes 786436
  42.7 4.0 %copy-start.7 = (s32[256,2]{0,1:T(2,128)S(1)}, s32[256,2]{0,1:T(2,128)}, u32[]{:S(2)}) copy-start(s32[256,2]{0,1:T(2,128)} %param.20) | copy-start | bytes 6148
  46.6 194.7 %all-gather.10.cloned.1.call-start = ((), (), s32[]{:S(2)}) async-start(), calls=%async_computation.5 | async-start | bytes 5242880 | tf_op jit(solution)/shard_map/all_gather | solution.py:133
  182.9 1.6 copy-start.10
  182.9 1.6 copy-start.14
  184.5 2.4 copy-start.11
  186.9 3.8 %copy-start.1 = (bf16[256,2048]{1,0:T(8,128)(2,1)S(1)}, bf16[256,2048]{1,0:T(8,128)(2,1)}, u32[]{:S(2)}) copy-start(bf16[256,2048]{1,0:T(8,128)(2,1)} %all-gather.6.cloned.1.call-done) | copy-start | bytes 3145732
  246.8 31.3 %all-to-all-start.2 = ((bf16[1,8,128,512]{3,2,0,1:T(8,128)(2,1)}), bf16[1,8,128,512]{3,2,0,1:T(8,128)(2,1)}, u32[]{:S(2)}, u32[]{:S(2)}) async-start(bf16[1,8,128,512]{3,2,0,1:T(8,128)(2,1)} %bitcast.93), calls=%async_computation.2 | async-start | bytes 2097152 | tf_op jit(solution)/shard_map/all_to_all | solution.py:140
  251.4 32.0 %all-gather.8.cloned.1.call-start = ((), (), s32[]{:S(2)}) async-start(), calls=%async_computation.4 | async-start | bytes 1310720 | tf_op jit(solution)/shard_map/all_gather | solution.py:134
  251.4 2.6 copy-start.12
  254.0 2.1 copy-start.8
  281.6 1.8 copy-start.3
Sparse Core Ops, SparseCore 0:
  46.7 25.0 all-gather.5
  190.8 50.3 all-gather.9
  255.8 26.7 all-gather.7
where the time goes:
time: 294 us; the launch traced here: 293 us
  blocking collectives  111 us (38%)
  waiting for transfers between devices  92.4 us (31%)
  local copies, waits for them, and re-layouts  30.1 us (10%)
  matrix products  25.3 us (9%)
  between operations  13.5 us (5%)
  starting transfers between devices  12.4 us (4%)
  other arithmetic  8.46 us (3%)
    all_to_all x1, blocking collectives, per_device(): lax.all_to_all(picked_rows.reshape(EXP_DEV, sp_count, capacity, stream_ro...  98.4 us
    all_gather x1, waiting for transfers between devices, per_device(): routed_piece = lax.all_gather(hidden, 'tp', axis=2, tiled=True)  50.3 us
    all_to_all x1, waiting for transfers between devices, per_device(): lax.all_to_all(outgoing, 'sp', split_axis=1, concat_axis=1, tiled=True)  21.8 us
    all_gather x1, waiting for transfers between devices, per_device(): stream_rows = lax.all_gather(stream_cols, 'tp', axis=1, tiled=True)  20.4 us
    all_gather x1, blocking collectives, per_device(): attended_all = lax.all_gather(attended_values, 'tp', axis=1, tiled=True)  12.7 us
    gather x1, local copies, waits for them, and re-layouts, per_device(): jnp.take(stream_rows, slot_owner, axis=0, mode='fill', fill_value=0)  10.2 us
  transfers between devices with their start and end apart: 6, of which 3 were waited for; matrix products, arithmetic and copies ran while one was open for 10% of the time, Pallas kernels for 0%

commit v1 on v0

--- a/solution.py
+++ b/solution.py
@@ -12,6 +12,12 @@
 EXP_DEV = 1
 TOK_DEV = 256
 norm_eps = 1e-06
+
+
+def exchange_blocks(x, name, split, join):
+    pieces = jnp.split(x, lax.axis_size(name), axis=split)
+    received = lax.all_to_all(jnp.stack(pieces), name, 0, 0)
+    return jnp.concatenate(received, axis=join)
 
 
 def passed_along(value, axis, steps):
@@ -110,12 +116,8 @@
         jnp.full((EXP_DEV * rows_per_expert,), TOK_DEV, jnp.int32).at[slot_index].set(token_of)
     )
     picked_rows = jnp.take(stream_rows, slot_owner, axis=0, mode="fill", fill_value=0)
-    arrived = lax.all_to_all(
-        picked_rows.reshape(EXP_DEV, sp_count, capacity, stream_rows.shape[1]),
-        "sp",
-        split_axis=1,
-        concat_axis=1,
-        tiled=True,
+    arrived = exchange_blocks(
+        picked_rows.reshape(EXP_DEV, sp_count, capacity, stream_rows.shape[1]), "sp", 1, 1
     )
     arrived = arrived.reshape(EXP_DEV, rows_per_expert, D)
     routed_squares = jnp.sum(jnp.square(arrived.astype(jnp.float32)), axis=-1)

time: 294 us -> 295 us (level)
  no operation moved by 1% of the time
where the time goes in v1:
time: 295 us; the launch traced here: 294 us
  blocking collectives  111 us (38%)
  waiting for transfers between devices  91.9 us (31%)
  local copies, waits for them, and re-layouts  31 us (11%)
  matrix products  26.2 us (9%)
  between operations  13.5 us (5%)
  starting transfers between devices  12.3 us (4%)
  other arithmetic  8.42 us (3%)
    all_to_all x1, blocking collectives, exchange_blocks(): received = lax.all_to_all(jnp.stack(pieces), name, 0, 0)  98.4 us
    all_gather x1, waiting for transfers between devices, per_device(): routed_piece = lax.all_gather(hidden, 'tp', axis=2, tiled=True)  50.3 us
    all_to_all x1, waiting for transfers between devices, per_device(): lax.all_to_all(outgoing, 'sp', split_axis=1, concat_axis=1, tiled=True)  21.2 us
    all_gather x1, waiting for transfers between devices, per_device(): stream_rows = lax.all_gather(stream_cols, 'tp', axis=1, tiled=True)  20.4 us
    all_gather x1, blocking collectives, per_device(): attended_all = lax.all_gather(attended_values, 'tp', axis=1, tiled=True)  12.8 us
    gather x1, local copies, waits for them, and re-layouts, per_device(): jnp.take(stream_rows, slot_owner, axis=0, mode='fill', fill_value=0)  10.2 us
  transfers between devices with their start and end apart: 6, of which 3 were waited for; matrix products, arithmetic and copies ran while one was open for 10% of the time, Pallas kernels for 0%

profile of v1, /device:TPU:0, one launch (start us, length us, event | category | flops | bytes accessed | tf_op | source)
XLA Modules:
  0.0 294.4 jit_solution(4029410759388592115)
XLA Ops:
  7.8 3.1 %collective-permute-start = (bf16[2,128,256]{1,2,0:T(8,128)(2,1)S(1)}, bf16[2,128,256]{1,2,0:T(8,128)(2,1)}, u32[]{:S(2)}, u32[]{:S(2)}) collective-permute-start(bf16[2,128,256]{1,2,0:T(8,128)(2,1)S(1)} %slice.34), channel_id=1, source_target_pairs={{0,4},{4,8},{8,12},{12,16},{16,20},{20,24},{24,28},{1,5},{5,9},{9,... | collective-permute-start | bytes 393224 | tf_op jit(solution)/shard_map/ppermute | solution.py:26
  10.9 2.2 copy.72
  13.1 4.5 %all-to-all-start = ((bf16[256,4,512]{0,2,1:T(8,128)(2,1)}), bf16[256,4,512]{0,2,1:T(8,128)(2,1)S(1)}, u32[]{:S(2)}, u32[]{:S(2)}) async-start(bf16[256,4,512]{0,2,1:T(8,128)(2,1)} %bitcast.121), calls=%async_computation | async-start | bytes 2097152 | tf_op jit(solution)/shard_map/all_to_all | solution.py:87
  20.5 1.4 gather_fusion
  27.5 1.4 fusion.56
  30.7 12.8 %all_gather.12 = bf16[256,1024]{0,1:T(8,128)(2,1)} all-gather(bf16[256,256]{0,1:T(8,128)(2,1)S(1)} %bitcast.125), channel_id=1, replica_groups=mesh['sp'=8,'tp'=4] {'tp'}, dimensions={1}, use_global_device_ids=true | all-gather | bytes 655360 | tf_op jit(solution)/shard_map/all_gather | solution.py:85
  43.4 1.3 copy.73
  44.8 2.6 fusion.25
  49.6 2.4 scatter_custom_fusion
  52.1 20.4 %all-gather.6.cloned.1.call-done = bf16[256,2048]{1,0:T(8,128)(2,1)} async-done(((bf16[256,512]{1,0:T(8,128)(2,1)}), bf16[256,2048]{1,0:T(8,128)(2,1)}) %all-gather.6.cloned.1.call-update) | async-done | bytes 1048592 | tf_op jit(solution)/shard_map/all_gather | solution.py:97
  72.5 10.2 %gather_fusion.1 = bf16[1024,2048]{1,0:T(8,128)(2,1)} fusion(bf16[256,2048]{1,0:T(8,128)(2,1)} %all-gather.6.cloned.1.call-done, s32[1024]{0:T(1024)S(1)} %fusion.47), kind=kCustom, calls=%fused_computation.1 | custom fusion | bytes 8392704 | tf_op jit(solution)/shard_map/jit(_take)/gather | solution.py:118
  82.6 2.5 broadcast_select_fusion
  85.5 98.4 %all_to_all.25 = bf16[8,1,1,128,2048]{4,3,2,1,0:T(8,128)(2,1)S(1)} all-to-all(bf16[8,1,1,128,2048]{4,3,2,1,0:T(8,128)(2,1)S(1)} %fusion.30), channel_id=1, replica_groups=mesh['sp'=8,'tp'=4] {'sp'}, dimensions={0} | all-to-all | bytes 8388608 | tf_op jit(solution)/shard_map/all_to_all | solution.py:19
  185.5 2.4 fusion.3
  188.0 3.7 %multiply_convert_fusion.6 = bf16[1024,512]{1,0:T(8,128)(2,1)} fusion(f32[1024,512]{1,0:T(8,128)S(1)} %fusion.3, bf16[1024,2048]{1,0:T(8,128)(2,1)S(1)} %bitcast.119, bf16[1,2048,512]{2,1,0:T(8,128)(2,1)S(1)} %copy-done.9, f32[2048]{0:T(1024)S(1)} %copy-done.12, f32[1024]{0:T(1024)S(1)} %rsqrt_bitcast_fusion), kind=kOutput, calls=%fused_computation.18 | convolution fusion | flops 2154823680 | bytes 9449472 | tf_op jit(solution)/shard_map/erd,edf->erf/dot_general | solution.py:125
  192.1 50.3 %all-gather.10.cloned.1.call-done = bf16[1024,2048]{1,0:T(8,128)(2,1)} async-done(((bf16[1024,512]{1,0:T(8,128)(2,1)}), bf16[1024,2048]{1,0:T(8,128)(2,1)}) %all-gather.10.cloned.1.call-update) | async-done | bytes 4194320 | tf_op jit(solution)/shard_map/all_gather | solution.py:135
  242.3 5.5 %fusion.16 = bf16[1024,512]{1,0:T(8,128)(2,1)} fusion(bf16[1024,2048]{1,0:T(8,128)(2,1)} %all-gather.10.cloned.1.call-done, bf16[1,2048,512]{2,1,0:T(8,128)(2,1)S(1)} %copy-done), kind=kOutput, calls=%fused_computation.24 | convolution fusion | flops 2148007936 | bytes 7340032 | tf_op jit(solution)/shard_map/erf,efd->erd/dot_general | solution.py:137
  247.8 4.6 %all-to-all-start.2 = ((bf16[1,8,128,512]{3,2,0,1:T(8,128)(2,1)}), bf16[1,8,128,512]{3,2,0,1:T(8,128)(2,1)}, u32[]{:S(2)}, u32[]{:S(2)}) async-start(bf16[1,8,128,512]{3,2,0,1:T(8,128)(2,1)} %bitcast.123), calls=%async_computation.2 | async-start | bytes 2097152 | tf_op jit(solution)/shard_map/all_to_all | solution.py:142
  252.5 2.6 fusion.23
  255.1 1.6 fusion.27
  257.9 21.2 %all-to-all-done.2 = bf16[1,8,128,512]{3,2,0,1:T(8,128)(2,1)} async-done(((bf16[1,8,128,512]{3,2,0,1:T(8,128)(2,1)}), bf16[1,8,128,512]{3,2,0,1:T(8,128)(2,1)}, u32[]{:S(2)}, u32[]{:S(2)}) %all-to-all-start.2) | async-done | bytes 1048608 | tf_op jit(solution)/shard_map/all_to_all | solution.py:142
  279.1 3.4 %gather_fusion.2 = bf16[512,512]{1,0:T(8,128)(2,1)S(1)} fusion(bf16[1024,512]{1,0:T(8,128)(2,1)} %bitcast.32, s32[1024]{0:T(1024)S(1)} %pad_clamp_fusion), kind=kCustom, calls=%fused_computation.2 | custom fusion | bytes 1050624 | tf_op jit(solution)/shard_map/jit(_take)/gather | solution.py:145
  282.7 1.8 fusion.38
  284.5 3.3 %fusion.26 = bf16[256,512]{1,0:T(8,128)(2,1)} fusion(bf16[256,2048]{1,0:T(8,128)(2,1)} %all-gather.8.cloned.1.call-done, bf16[2048,512]{1,0:T(8,128)(2,1)} %param.27, f32[256,1,512]{2,1,0:T(1,128)S(1)} %fusion.38, bf16[256,512]{1,0:T(8,128)(2,1)S(1)} %copy-done.3), kind=kOutput, calls=%fused_computation.35 | convolution fusion | flops 537395200 | bytes 4194304 | tf_op jit(solution)/shard_map/dot_general | solution.py:140
  (94 shorter events, 17.4 us)
Async XLA Ops:
  6.5 235.8 %copy-start = (bf16[1,2048,512]{2,1,0:T(8,128)(2,1)S(1)}, bf16[1,2048,512]{2,1,0:T(8,128)(2,1)}, u32[]{:S(2)}) copy-start(bf16[1,2048,512]{2,1,0:T(8,128)(2,1)} %param.24) | copy-start | bytes 6291460
  6.5 12.1 %copy-start.4 = (bf16[256,256]{1,0:T(8,128)(2,1)S(1)}, bf16[256,256]{1,0:T(8,128)(2,1)}, u32[]{:S(2)}) copy-start(bf16[256,256]{1,0:T(8,128)(2,1)} %param.14) | copy-start | bytes 393220
  7.8 5.3 %copy-start.2 = (bf16[2,256,256]{1,2,0:T(8,128)(2,1)}, bf16[2,256,256]{1,2,0:T(8,128)(2,1)S(1)}, u32[]{:S(2)}) copy-start(bf16[2,256,256]{1,2,0:T(8,128)(2,1)S(1)} %copy.62) | copy-start | bytes 786436
  7.8 11.7 %collective-permute-start = (bf16[2,128,256]{1,2,0:T(8,128)(2,1)S(1)}, bf16[2,128,256]{1,2,0:T(8,128)(2,1)}, u32[]{:S(2)}, u32[]{:S(2)}) collective-permute-start(bf16[2,128,256]{1,2,0:T(8,128)(2,1)S(1)} %slice.34), channel_id=1, source_target_pairs={{0,4},{4,8},{8,12},{12,16},{16,20},{20,24},{24,28},{1,5},{5,9},{9,... | collective-permute-start | bytes 393224 | tf_op jit(solution)/shard_map/ppermute | solution.py:26
  13.1 30.3 %all-to-all-start = ((bf16[256,4,512]{0,2,1:T(8,128)(2,1)}), bf16[256,4,512]{0,2,1:T(8,128)(2,1)S(1)}, u32[]{:S(2)}, u32[]{:S(2)}) async-start(bf16[256,4,512]{0,2,1:T(8,128)(2,1)} %bitcast.121), calls=%async_computation | async-start | bytes 2097152 | tf_op jit(solution)/shard_map/all_to_all | solution.py:87
  17.7 54.8 %all-gather.6.cloned.1.call-start = ((), (), s32[]{:S(2)}) async-start(), calls=%async_computation.3 | async-start | bytes 1310720 | tf_op jit(solution)/shard_map/all_gather | solution.py:97
  18.6 10.3 %copy-start.7 = (f32[4]{0:T(128)S(1)}, f32[4]{0:T(128)}, u32[]{:S(2)}) copy-start(f32[4]{0:T(128)} %param.16) | copy-start | bytes 52
  29.0 15.8 %copy-start.11 = (bf16[256,512]{1,0:T(8,128)(2,1)S(1)}, bf16[256,512]{1,0:T(8,128)(2,1)}, u32[]{:S(2)}) copy-start(bf16[256,512]{1,0:T(8,128)(2,1)} %param.18) | copy-start | bytes 786436
  29.2 18.2 %copy-start.5 = (s32[256,2]{0,1:T(2,128)S(1)}, s32[256,2]{0,1:T(2,128)}, u32[]{:S(2)}) copy-start(s32[256,2]{0,1:T(2,128)} %param.20) | copy-start | bytes 6148
  47.3 195.0 %all-gather.10.cloned.1.call-start = ((), (), s32[]{:S(2)}) async-start(), calls=%async_computation.5 | async-start | bytes 5242880 | tf_op jit(solution)/shard_map/all_gather | solution.py:135
  183.9 1.6 copy-start.8
  183.9 1.6 copy-start.12
  185.5 2.4 copy-start.9
  188.0 3.8 %copy-start.1 = (bf16[256,2048]{1,0:T(8,128)(2,1)S(1)}, bf16[256,2048]{1,0:T(8,128)(2,1)}, u32[]{:S(2)}) copy-start(bf16[256,2048]{1,0:T(8,128)(2,1)} %all-gather.6.cloned.1.call-done) | copy-start | bytes 3145732
  247.8 31.3 %all-to-all-start.2 = ((bf16[1,8,128,512]{3,2,0,1:T(8,128)(2,1)}), bf16[1,8,128,512]{3,2,0,1:T(8,128)(2,1)}, u32[]{:S(2)}, u32[]{:S(2)}) async-start(bf16[1,8,128,512]{3,2,0,1:T(8,128)(2,1)} %bitcast.123), calls=%async_computation.2 | async-start | bytes 2097152 | tf_op jit(solution)/shard_map/all_to_all | solution.py:142
  252.4 32.1 %all-gather.8.cloned.1.call-start = ((), (), s32[]{:S(2)}) async-start(), calls=%async_computation.4 | async-start | bytes 1310720 | tf_op jit(solution)/shard_map/all_gather | solution.py:136
  252.4 2.6 copy-start.10
  255.0 2.7 copy-start.6
  279.1 5.4 %copy-start.3 = (bf16[256,512]{1,0:T(8,128)(2,1)S(1)}, bf16[256,512]{1,0:T(8,128)(2,1)}, u32[]{:S(2)}) copy-start(bf16[256,512]{1,0:T(8,128)(2,1)} %fusion.25) | copy-start | bytes 786436
Sparse Core Ops, SparseCore 0:
  47.4 24.9 all-gather.5
  191.9 50.3 all-gather.9
  256.8 26.7 all-gather.7
